TPU v7x, 32 devices: a whole 2x2x4 slice. The times are simulated.
32 devices in a mesh: kv: 8 (over z, y), tp: 4 (over x, core).
Axes of the slice: x: 2, y: 2, z: 4, core: 2. Of those that a mesh axis runs over, the one named last changes fastest.
Arguments:
- tokens: bfloat16 [4096, 2048], P('kv'), may hold values from -18 to 18
- w_query: bfloat16 [2048, 1024], P(None, 'tp'), may hold values from -0.125 to 0.125
- w_key: bfloat16 [2048, 256], P(None, 'tp'), may hold values from -0.125 to 0.125
- w_value: bfloat16 [2048, 256], P(None, 'tp'), may hold values from -18 to 18
- w_out: bfloat16 [1024, 2048], P(None, 'tp'), may hold values from -0.1875 to 0.1875
- out_gain: float32 [1024], replicated, may hold values from 0.1 to 1.9
- chosen: int32 [4, 64, 8], P('tp', 'kv'), may hold values from -1 to 63, as said below
Outputs:
- mixed_out: bfloat16 [4096, 2048], P('kv', 'tp')
Inputs may be any that keep to these rules, and one draw needn't show every extreme that they name: chosen[h, b, 0] is b itself; the other entries of a row are distinct key blocks lying wholly before block b, or -1, placed after all named blocks; for each key head h, the query blocks on one index of kv (its 512 positions) name, together, at most one key block of head h held by any other index of kv.
All inputs are finite; a program needn't handle non-finite values.
Results may differ from a plain program's by a relative error of at most 0.024.
Values may be sent and summed in bfloat16 or wider, within the bound.
A program may use at most 64 MiB of HBM per device.

v0:
```python
import jax
import jax.numpy as jnp
from jax import lax
from jax.sharding import PartitionSpec as P

HQ = 16
HD = 64
BLK = 64
SEL = 8


rope_base = 500000.0
norm_eps = 1e-06


def rotate(vectors, positions):
    half_size = vectors.shape[-1] // 2
    frequency = rope_base ** (-jnp.arange(half_size, dtype=jnp.float32) / half_size)
    angles = positions.astype(jnp.float32)[:, None] * frequency[None, :]
    cosine = jnp.cos(angles)[:, None, :]
    sine_wave = jnp.sin(angles)[:, None, :]
    lower_half = vectors[..., :half_size]
    upper_half = vectors[..., half_size:]
    return jnp.concatenate(
        [
            lower_half * cosine - upper_half * sine_wave,
            upper_half * cosine + lower_half * sine_wave,
        ],
        axis=-1,
    )


def per_device(tokens, w_query, w_key, w_value, w_out, out_gain, chosen):
    count_kv = lax.axis_size("kv")
    kv_place = lax.axis_index("kv")
    row_count = tokens.shape[0]
    block_count = row_count // BLK
    feat_width = w_query.shape[1]
    head_count = feat_width // HD
    positions = kv_place * row_count + jnp.arange(row_count, dtype=jnp.int32)
    queries = rotate(
        jnp.dot(tokens, w_query, preferred_element_type=jnp.float32).reshape(
            row_count, head_count, HD
        ),
        positions,
    ).astype(jnp.bfloat16)
    key_rows = (
        rotate(
            jnp.dot(tokens, w_key, preferred_element_type=jnp.float32).reshape(row_count, 1, HD),
            positions,
        )
        .astype(jnp.bfloat16)
        .reshape(row_count, HD)
    )
    value_rows = jnp.dot(tokens, w_value, preferred_element_type=jnp.float32).astype(jnp.bfloat16)
    local_pairs = jnp.concatenate([key_rows, value_rows], axis=1).reshape(block_count, BLK, 2 * HD)
    chosen_ids = chosen[0]
    usable = chosen_ids >= 0
    owners = jnp.where(usable, chosen_ids // block_count, kv_place)
    local_index = jnp.where(usable, chosen_ids % block_count, 0)
    remote = usable & (owners != kv_place)
    peer_ids = jnp.arange(count_kv, dtype=jnp.int32)
    matches = remote[:, :, None] & (owners[:, :, None] == peer_ids[None, None, :])
    wanted = jnp.max(jnp.where(matches, local_index[:, :, None], -1), axis=(0, 1))
    asked_for = lax.all_to_all(
        wanted.reshape(count_kv, 1), "kv", split_axis=0, concat_axis=0, tiled=True
    )[:, 0]
    outgoing = jnp.where(
        (asked_for >= 0)[:, None, None],
        local_pairs[jnp.maximum(asked_for, 0)],
        jnp.zeros((), jnp.bfloat16),
    )
    arrived = lax.all_to_all(outgoing, "kv", split_axis=0, concat_axis=0, tiled=True)
    pool_pairs = jnp.concatenate([arrived, local_pairs], axis=0)
    slot_index = jnp.where(owners == kv_place, count_kv + local_index, owners)
    selected = pool_pairs[slot_index]
    pair_count = block_count // 2
    offsets = jnp.arange(BLK, dtype=jnp.int32)
    score_scale = HD ** (-0.5)

    def attend(bundle):
        query_part, stacked, pair_ids, pair_usable, query_pos = bundle
        key_part = stacked[..., :HD]
        value_part = stacked[..., HD:]
        scores = (
            jnp.einsum("pqhd,pskd->phqsk", query_part, key_part, preferred_element_type=jnp.float32)
            * score_scale
        )
        key_pos = pair_ids[:, :, None] * BLK + offsets
        allowed = pair_usable[:, None, :, None] & (
            key_pos[:, None, :, :] <= query_pos[:, :, None, None]
        )
        scores = jnp.where(allowed[:, None], scores, -jnp.inf)
        peak_score = jnp.max(scores, axis=(3, 4), keepdims=True)
        weights = jnp.exp(scores - peak_score)
        softmax_w = (weights / jnp.sum(weights, axis=(3, 4), keepdims=True)).astype(jnp.bfloat16)
        mixed_out = jnp.einsum(
            "phqsk,pskd->pqhd", softmax_w, value_part, preferred_element_type=jnp.float32
        )
        return mixed_out.astype(jnp.bfloat16)

    attended = lax.map(
        attend,
        (
            queries.reshape(pair_count, 2, BLK, head_count, HD),
            selected.reshape(pair_count, 2, SEL, BLK, 2 * HD),
            chosen_ids.reshape(pair_count, 2, SEL),
            usable.reshape(pair_count, 2, SEL),
            positions.reshape(pair_count, 2, BLK),
        ),
    ).reshape(row_count, feat_width)
    attn_f32 = attended.astype(jnp.float32)
    squares = lax.psum(jnp.sum(attn_f32 * attn_f32, axis=1), "tp")
    gain_part = lax.dynamic_slice_in_dim(out_gain, lax.axis_index("tp") * feat_width, feat_width)
    scaled = (attn_f32 * gain_part[None, :]).astype(jnp.bfloat16)
    product = jnp.dot(
        lax.all_gather(scaled, "tp", axis=1, tiled=True), w_out, preferred_element_type=jnp.float32
    )
    inverse = lax.rsqrt(squares / (HQ * HD) + norm_eps)
    return (inverse[:, None] * product).astype(jnp.bfloat16)


def solution(mesh):
    return jax.shard_map(
        per_device,
        mesh=mesh,
        in_specs=(
            P("kv", None),
            P(None, "tp"),
            P(None, "tp"),
            P(None, "tp"),
            P(None, "tp"),
            P(),
            P("tp", "kv", None),
        ),
        out_specs=P("kv", "tp"),
        check_vma=False,
    )
```

profile of v0, /device:TPU:0, one launch (start us, length us, event | category | flops | bytes accessed | tf_op | source)
XLA Modules:
  0.0 87.1 jit_solution(12271367534152278380)
XLA Ops:
  6.5 0.8 fusion.20
  7.4 0.7 compare_and_fusion.1
  8.2 0.7 copy.36
  8.9 7.3 %all-to-all-start = ((s32[8,1,1]{2,1,0:T(1,128)}), s32[8,1,1]{2,1,0:T(1,128)S(1)}, u32[]{:S(2)}, u32[]{:S(2)}) async-start(s32[8,1,1]{2,1,0:T(1,128)} %copy.36), calls=%async_computation | async-start | bytes 8192 | tf_op jit(solution)/shard_map/all_to_all | solution.py:65
  16.2 0.7 compare_select_fusion
  16.9 1.7 %convolution_bitcast_fusion.1 = f32[512,1,64]{0,2,1:T(8,128)S(1)} fusion(bf16[512,2048]{1,0:T(8,128)(2,1)S(1)} %copy-done, bf16[2048,64]{0,1:T(8,128)(2,1)} %param.11), kind=kOutput, calls=%fused_computation.26 | convolution fusion | flops 134217728 | bytes 2490368 | tf_op jit(solution)/shard_map/dot_general | solution.py:49
  19.6 0.8 convolution_convert_fusion
  20.4 2.0 %fusion.34 = f32[512,256]{0,1:T(8,128)S(1)} fusion(bf16[512,2048]{1,0:T(8,128)(2,1)S(1)} %copy-done, bf16[2048,256]{1,0:T(8,128)(2,1)} %param.10), kind=kOutput, calls=%fused_computation.93 | convolution fusion | flops 536870912 | bytes 3670016 | tf_op jit(solution)/shard_map/dot_general | solution.py:42
  22.9 1.6 %pad_maximum_fusion = bf16[4,2,64,4,64]{2,1,0,4,3:T(2,128)(2,1)} fusion(bf16[4,2,64,4,32]{2,1,0,4,3:T(2,128)(2,1)S(1)} %concatenate.35, bf16[4,2,64,4,32]{2,1,0,4,3:T(2,128)(2,1)S(1)} %concatenate.34), kind=kLoop, calls=%fused_computation.29 | loop fusion | flops 131072 | bytes 524288 | tf_op jit(solution)/shard_map/concatenate | solution.py:24
  25.9 0.7 broadcast_select_fusion
  26.6 6.0 %all-to-all-start.1 = ((bf16[8,64,128]{2,1,0:T(8,128)(2,1)}), bf16[8,64,128]{2,1,0:T(8,128)(2,1)S(1)}, u32[]{:S(2)}, u32[]{:S(2)}) async-start(bf16[8,64,128]{2,1,0:T(8,128)(2,1)} %broadcast_select_fusion), calls=%async_computation.1 | async-start | bytes 262144 | tf_op jit(solution)/shard_map/all_to_all | solution.py:73
  32.7 0.8 dynamic_slice.23
  33.4 6.5 %all-to-all-done.1 = bf16[8,64,128]{2,1,0:T(8,128)(2,1)S(1)} async-done(((bf16[8,64,128]{2,1,0:T(8,128)(2,1)}), bf16[8,64,128]{2,1,0:T(8,128)(2,1)S(1)}, u32[]{:S(2)}, u32[]{:S(2)}) %all-to-all-start.1) | async-done | bytes 131104 | tf_op jit(solution)/shard_map/all_to_all | solution.py:73
  40.1 0.7 gather_fusion.1
  40.8 17.1 %while.11 = (s32[]{:T(128)}, bf16[4,2,64,4,64]{2,4,3,1,0:T(8,128)(2,1)}, bf16[4,2,8,64,128]{4,3,2,1,0:T(8,128)(2,1)S(1)}, pred[4,2,8]{2,1,0:T(4,128)(4,1)S(1)}, ...) while((s32[]{:T(128)}, ...), condition=%wide.region_4.5_spmd.clone, body=%wide.region_1.4_spmd.clone.sunk | while | flops 69369872 | bytes 13193617 | solution.py:102
  41.8 1.0 %constant_dynamic-slice_fusion.4 = bf16[1,2,64,4,64]{2,1,0,4,3:T(2,128)(2,1)S(1)} fusion(bf16[4,2,64,4,64]{2,1,0,4,3:T(2,128)(2,1)} %get-tuple-element.185, s32[]{:T(128)} %get-tuple-element.171), kind=kLoop, calls=%fused_computation.18.clone.1 | loop fusion | bytes 131076 | tf_op jit(solution)/shard_map/while/body/jit(dynamic_index_in_dim)/dynamic_slice | solution.py:102
  43.9 1.2 %fusion.52 = bf16[4,2,64,4,64]{2,4,3,1,0:T(8,128)(2,1)} fusion(bf16[4,2,64,4,64]{2,4,3,1,0:T(8,128)(2,1)} %get-tuple-element.172, s32[]{:T(128)} %get-tuple-element.171, f32[2,4,64,8,64]{2,4,1,3,0:T(8,128)S(1)} %get-tuple-element.161, f32[2,4,64]{2,1,0:T(4,128)S(1)} %fusion.51, f32[2,4,64]{2,1,0:T(4,128)S(1)} %get-tuple-element.162, ...), kind=kOutput, calls=%fused_computation.10.clone.1 | convolution fusion | flops 34373632 | bytes 1446400 | tf_op jit(solution)/shard_map/while/body/eval_jaxpr/phqsk,pskd->pqhd/dot_general | solution.py:97
  45.5 0.6 copy-done.1
  46.1 1.0 %constant_dynamic-slice_fusion.4 = bf16[1,2,64,4,64]{2,1,0,4,3:T(2,128)(2,1)S(1)} fusion(bf16[4,2,64,4,64]{2,1,0,4,3:T(2,128)(2,1)} %get-tuple-element.185, s32[]{:T(128)} %get-tuple-element.171), kind=kLoop, calls=%fused_computation.18.clone.1 | loop fusion | bytes 131076 | tf_op jit(solution)/shard_map/while/body/jit(dynamic_index_in_dim)/dynamic_slice | solution.py:102
  48.1 1.2 %fusion.52 = bf16[4,2,64,4,64]{2,4,3,1,0:T(8,128)(2,1)} fusion(bf16[4,2,64,4,64]{2,4,3,1,0:T(8,128)(2,1)} %get-tuple-element.172, s32[]{:T(128)} %get-tuple-element.171, f32[2,4,64,8,64]{2,4,1,3,0:T(8,128)S(1)} %get-tuple-element.161, f32[2,4,64]{2,1,0:T(4,128)S(1)} %fusion.51, f32[2,4,64]{2,1,0:T(4,128)S(1)} %get-tuple-element.162, ...), kind=kOutput, calls=%fused_computation.10.clone.1 | convolution fusion | flops 34373632 | bytes 1446400 | tf_op jit(solution)/shard_map/while/body/eval_jaxpr/phqsk,pskd->pqhd/dot_general | solution.py:97
  50.4 1.0 %constant_dynamic-slice_fusion.4 = bf16[1,2,64,4,64]{2,1,0,4,3:T(2,128)(2,1)S(1)} fusion(bf16[4,2,64,4,64]{2,1,0,4,3:T(2,128)(2,1)} %get-tuple-element.185, s32[]{:T(128)} %get-tuple-element.171), kind=kLoop, calls=%fused_computation.18.clone.1 | loop fusion | bytes 131076 | tf_op jit(solution)/shard_map/while/body/jit(dynamic_index_in_dim)/dynamic_slice | solution.py:102
  52.4 1.2 %fusion.52 = bf16[4,2,64,4,64]{2,4,3,1,0:T(8,128)(2,1)} fusion(bf16[4,2,64,4,64]{2,4,3,1,0:T(8,128)(2,1)} %get-tuple-element.172, s32[]{:T(128)} %get-tuple-element.171, f32[2,4,64,8,64]{2,4,1,3,0:T(8,128)S(1)} %get-tuple-element.161, f32[2,4,64]{2,1,0:T(4,128)S(1)} %fusion.51, f32[2,4,64]{2,1,0:T(4,128)S(1)} %get-tuple-element.162, ...), kind=kOutput, calls=%fused_computation.10.clone.1 | convolution fusion | flops 34373632 | bytes 1446400 | tf_op jit(solution)/shard_map/while/body/eval_jaxpr/phqsk,pskd->pqhd/dot_general | solution.py:97
  54.0 0.6 copy-done.1
  54.7 1.0 %constant_dynamic-slice_fusion.4 = bf16[1,2,64,4,64]{2,1,0,4,3:T(2,128)(2,1)S(1)} fusion(bf16[4,2,64,4,64]{2,1,0,4,3:T(2,128)(2,1)} %get-tuple-element.185, s32[]{:T(128)} %get-tuple-element.171), kind=kLoop, calls=%fused_computation.18.clone.1 | loop fusion | bytes 131076 | tf_op jit(solution)/shard_map/while/body/jit(dynamic_index_in_dim)/dynamic_slice | solution.py:102
  56.7 1.2 %fusion.52 = bf16[4,2,64,4,64]{2,4,3,1,0:T(8,128)(2,1)} fusion(bf16[4,2,64,4,64]{2,4,3,1,0:T(8,128)(2,1)} %get-tuple-element.172, s32[]{:T(128)} %get-tuple-element.171, f32[2,4,64,8,64]{2,4,1,3,0:T(8,128)S(1)} %get-tuple-element.161, f32[2,4,64]{2,1,0:T(4,128)S(1)} %fusion.51, f32[2,4,64]{2,1,0:T(4,128)S(1)} %get-tuple-element.162, ...), kind=kOutput, calls=%fused_computation.10.clone.1 | convolution fusion | flops 34373632 | bytes 1446400 | tf_op jit(solution)/shard_map/while/body/eval_jaxpr/phqsk,pskd->pqhd/dot_general | solution.py:97
  57.9 1.3 %copy.41 = f32[4,2,64,4,64]{4,3,2,1,0:T(4,128)S(1)} copy(bf16[4,2,64,4,64]{2,4,3,1,0:T(8,128)(2,1)} %get-tuple-element.47) | data formatting | bytes 786432 | tf_op jit(solution)/shard_map/convert_element_type | solution.py:112
  59.3 1.4 %reshape.350 = f32[512,256]{1,0:T(8,128)} reshape(f32[4,2,64,4,64]{4,3,2,1,0:T(4,128)S(1)} %copy.41) | data formatting | bytes 1048576 | tf_op jit(solution)/shard_map/convert_element_type | solution.py:112
  60.7 1.8 %multiply_convert_fusion = bf16[512,256]{1,0:T(8,128)(2,1)} fusion(f32[512,256]{1,0:T(8,128)} %reshape.350, f32[256]{0:T(256)S(1)} %dynamic_slice.23), kind=kLoop, calls=%fused_computation.30 | loop fusion | flops 262144 | bytes 787456 | tf_op jit(solution)/shard_map/convert_element_type | solution.py:115
  62.5 1.2 %multiply_reduce_fusion = f32[4,2,64]{2,1,0:T(2,128)S(1)} fusion(bf16[4,2,64,4,64]{2,4,3,1,0:T(8,128)(2,1)} %get-tuple-element.47), kind=kLoop, calls=%fused_computation.28 | loop fusion | flops 392704 | bytes 264192 | tf_op jit(solution)/shard_map/reduce_sum | solution.py:113
  63.8 5.6 %psum.7 = f32[512]{0:T(512)S(1)} all-reduce(f32[512]{0:T(512)S(1)} %reduce_sum.21), channel_id=1, replica_groups=mesh['kv'=8,'tp'=4] {'tp'}, use_global_device_ids=true, to_apply=%region_6.7 | all-reduce | flops 512 | bytes 4096 | tf_op jit(solution)/shard_map/psum | solution.py:113
  69.4 7.8 %all-gather.2.cloned.1.call-done = bf16[512,1024]{1,0:T(8,128)(2,1)} async-done(((bf16[512,256]{1,0:T(8,128)(2,1)}), bf16[512,1024]{1,0:T(8,128)(2,1)}) %all-gather.2.cloned.1.call-update) | async-done | bytes 1048592 | tf_op jit(solution)/shard_map/all_gather | solution.py:117
  77.3 3.0 %fusion.10 = bf16[512,512]{1,0:T(8,128)(2,1)} fusion(bf16[512,1024]{1,0:T(8,128)(2,1)} %all-gather.2.cloned.1.call-done, bf16[1024,512]{1,0:T(8,128)(2,1)} %param.13, f32[512]{0:T(512)S(1)} %add_rsqrt_fusion), kind=kOutput, calls=%fused_computation.25 | convolution fusion | flops 537395200 | bytes 2623488 | tf_op jit(solution)/shard_map/dot_general | solution.py:116
  (83 shorter events, 9.9 us)
Async XLA Ops:
  6.5 10.4 %copy-start = (bf16[512,2048]{1,0:T(8,128)(2,1)S(1)}, bf16[512,2048]{1,0:T(8,128)(2,1)}, u32[]{:S(2)}) copy-start(bf16[512,2048]{1,0:T(8,128)(2,1)} %param.9) | copy-start | bytes 6291460
  6.5 13.0 %copy-start.3 = (bf16[2048,64]{0,1:T(8,128)(2,1)S(1)}, bf16[2048,64]{0,1:T(8,128)(2,1)}, u32[]{:S(2)}) copy-start(bf16[2048,64]{0,1:T(8,128)(2,1)} %param.12) | copy-start | bytes 786436
  8.9 15.9 %all-to-all-start = ((s32[8,1,1]{2,1,0:T(1,128)}), s32[8,1,1]{2,1,0:T(1,128)S(1)}, u32[]{:S(2)}, u32[]{:S(2)}) async-start(s32[8,1,1]{2,1,0:T(1,128)} %copy.36), calls=%async_computation | async-start | bytes 8192 | tf_op jit(solution)/shard_map/all_to_all | solution.py:65
  22.4 11.0 %copy-start.4 = (s32[1,8,8]{2,1,0:T(8,128)S(1)}, s32[1,8,8]{2,1,0:T(8,128)}, u32[]{:S(2)}) copy-start(s32[1,8,8]{2,1,0:T(8,128)} %param.15) | copy-start | bytes 772
  26.6 13.3 %all-to-all-start.1 = ((bf16[8,64,128]{2,1,0:T(8,128)(2,1)}), bf16[8,64,128]{2,1,0:T(8,128)(2,1)S(1)}, u32[]{:S(2)}, u32[]{:S(2)}) async-start(bf16[8,64,128]{2,1,0:T(8,128)(2,1)} %broadcast_select_fusion), calls=%async_computation.1 | async-start | bytes 262144 | tf_op jit(solution)/shard_map/all_to_all | solution.py:73
  32.6 44.7 %all-gather.2.cloned.1.call-start = ((), (), s32[]{:S(2)}) async-start(), calls=%async_computation.2 | async-start | bytes 1310720 | tf_op jit(solution)/shard_map/all_gather | solution.py:117
  40.8 1.0 %copy-start.1 = (bf16[4,2,8,64,128]{4,3,2,1,0:T(8,128)(2,1)}, bf16[4,2,8,64,128]{4,3,2,1,0:T(8,128)(2,1)S(1)}, u32[]{:S(2)}) copy-start(bf16[4,2,8,64,128]{4,3,2,1,0:T(8,128)(2,1)S(1)} %get-tuple-element.181) | copy-start | bytes 3145732 | tf_op jit(solution)/shard_map/while
  43.9 1.2 %copy-start.2 = (bf16[4,2,8,64,128]{4,3,2,1,0:T(8,128)(2,1)S(1)}, bf16[4,2,8,64,128]{4,3,2,1,0:T(8,128)(2,1)}, u32[]{:S(2)}) copy-start(bf16[4,2,8,64,128]{4,3,2,1,0:T(8,128)(2,1)} %copy-done.1) | copy-start | bytes 3145732 | tf_op jit(solution)/shard_map/while
  45.1 1.0 %copy-start.1 = (bf16[4,2,8,64,128]{4,3,2,1,0:T(8,128)(2,1)}, bf16[4,2,8,64,128]{4,3,2,1,0:T(8,128)(2,1)S(1)}, u32[]{:S(2)}) copy-start(bf16[4,2,8,64,128]{4,3,2,1,0:T(8,128)(2,1)S(1)} %get-tuple-element.181) | copy-start | bytes 3145732 | tf_op jit(solution)/shard_map/while
  48.1 1.2 %copy-start.2 = (bf16[4,2,8,64,128]{4,3,2,1,0:T(8,128)(2,1)S(1)}, bf16[4,2,8,64,128]{4,3,2,1,0:T(8,128)(2,1)}, u32[]{:S(2)}) copy-start(bf16[4,2,8,64,128]{4,3,2,1,0:T(8,128)(2,1)} %copy-done.1) | copy-start | bytes 3145732 | tf_op jit(solution)/shard_map/while
  49.4 1.0 %copy-start.1 = (bf16[4,2,8,64,128]{4,3,2,1,0:T(8,128)(2,1)}, bf16[4,2,8,64,128]{4,3,2,1,0:T(8,128)(2,1)S(1)}, u32[]{:S(2)}) copy-start(bf16[4,2,8,64,128]{4,3,2,1,0:T(8,128)(2,1)S(1)} %get-tuple-element.181) | copy-start | bytes 3145732 | tf_op jit(solution)/shard_map/while
  52.4 1.2 %copy-start.2 = (bf16[4,2,8,64,128]{4,3,2,1,0:T(8,128)(2,1)S(1)}, bf16[4,2,8,64,128]{4,3,2,1,0:T(8,128)(2,1)}, u32[]{:S(2)}) copy-start(bf16[4,2,8,64,128]{4,3,2,1,0:T(8,128)(2,1)} %copy-done.1) | copy-start | bytes 3145732 | tf_op jit(solution)/shard_map/while
  53.7 1.0 %copy-start.1 = (bf16[4,2,8,64,128]{4,3,2,1,0:T(8,128)(2,1)}, bf16[4,2,8,64,128]{4,3,2,1,0:T(8,128)(2,1)S(1)}, u32[]{:S(2)}) copy-start(bf16[4,2,8,64,128]{4,3,2,1,0:T(8,128)(2,1)S(1)} %get-tuple-element.181) | copy-start | bytes 3145732 | tf_op jit(solution)/shard_map/while
  56.7 1.2 %copy-start.2 = (bf16[4,2,8,64,128]{4,3,2,1,0:T(8,128)(2,1)S(1)}, bf16[4,2,8,64,128]{4,3,2,1,0:T(8,128)(2,1)}, u32[]{:S(2)}) copy-start(bf16[4,2,8,64,128]{4,3,2,1,0:T(8,128)(2,1)} %copy-done.1) | copy-start | bytes 3145732 | tf_op jit(solution)/shard_map/while
Sparse Core Ops, SparseCore 0:
  62.6 14.5 all-gather.1
where the time goes:
time: 87.9 us; the launch traced here: 87.1 us
  matrix products  14.5 us (16%)
  waiting for transfers between devices  14.3 us (16%)
  local copies, waits for them, and re-layouts  13.6 us (15%)
  between operations  13.6 us (15%)
  starting transfers between devices  13.3 us (15%)
  other arithmetic  11.9 us (14%)
  blocking collectives  5.63 us (6%)
    all_gather x1, waiting for transfers between devices, per_device(): lax.all_gather(scaled, 'tp', axis=1, tiled=True)  7.83 us
    all_to_all x1, starting transfers between devices, per_device(): lax.all_to_all(wanted.reshape(count_kv, 1), 'kv', split_axis=0, concat_ax...  7.31 us
    all_to_all x1, waiting for transfers between devices, per_device(): lax.all_to_all(outgoing, 'kv', split_axis=0, concat_axis=0, tiled=True)  6.5 us
    all_to_all x1, starting transfers between devices, per_device(): lax.all_to_all(outgoing, 'kv', split_axis=0, concat_axis=0, tiled=True)  6 us
    psum x1, blocking collectives, per_device(): squares = lax.psum(jnp.sum(attn_f32 * attn_f32, axis=1), 'tp')  5.63 us
    dot_general x4, matrix products, attend(): jnp.einsum('phqsk,pskd->pqhd', softmax_w, value_part, preferred_element_t...  4.94 us
    dynamic_slice x8, local copies, waits for them, and re-layouts, per_device(): lax.map(attend, (queries.reshape(pair_count, 2, BLK, head_count, HD), sel...  4.53 us
    dot_general x1, matrix products, per_device(): jnp.dot(lax.all_gather(scaled, 'tp', axis=1, tiled=True), w_out, preferre...  3.04 us
  transfers between devices with their start and end apart: 3, of which 2 were waited for; matrix products, arithmetic and copies ran while one was open for 12% of the time, Pallas kernels for 0%

commit v1 on v0

v1 whole, which is shorter than its diff:
```python
import functools
import math

import jax
import jax.numpy as jnp
import numpy as np
from jax import lax
from jax.experimental import pallas as pl
from jax.experimental.pallas import tpu as pltpu
from jax.sharding import PartitionSpec as P

HD = 64
BLK = 64
ROPE_BASE = 500000.0
NORM_EPS = 1e-06
MASKED = -1e30
MESH = pl.DeviceIdType.MESH
F32 = jnp.float32
BF16 = jnp.bfloat16


def angle_tables(count, step):
    half = HD // 2
    lane = np.arange(2 * HD) % half
    frequency = ROPE_BASE ** (-lane.astype(np.float64) / half)
    angles = (np.arange(count, dtype=np.float64) * step)[:, None] * frequency[None, :]
    return np.cos(angles).astype(np.float32), np.sin(angles).astype(np.float32)


def kernel(
    n_kv,
    n_tp,
    tokens_hbm,
    wq_hbm,
    wk_hbm,
    wv_hbm,
    wo_hbm,
    gain_ref,
    chosen_smem,
    chosen_vmem,
    cos_block,
    sin_block,
    cos_row,
    sin_row,
    out_ref,
    tokens,
    wq,
    w_pair,
    wo,
    cos_tab,
    sin_tab,
    ask_out,
    asks,
    kv_local,
    kv_out,
    kv_in,
    k_pool,
    v_pool,
    q_stack,
    gathered,
    acc,
    sq_acc,
    load_sem,
    ask_send,
    ask_recv,
    kv_send,
    kv_recv,
    near_send,
    far_send,
    relay_send,
    g_recv,
):
    me = lax.axis_index("kv")
    tp = lax.axis_index("tp")
    rows = tokens.shape[0]
    blocks = rows // BLK
    sel = chosen_smem.shape[1]
    feat = wq.shape[1]
    heads = feat // HD
    total_feat = wo.shape[0]
    null_id = n_kv + blocks
    parts = 2
    part = rows // parts

    partner = tp + 1 - 2 * lax.rem(tp, 2)
    far = [lax.rem(tp + 2 * k, n_tp) for k in range(1, n_tp // 2)]

    def peer_loop(body):
        if n_kv <= 8:
            for peer in range(n_kv):
                body(peer)
        else:

            @pl.loop(0, n_kv)
            def _(peer):
                body(peer)

    loads = [
        pltpu.make_async_copy(wk_hbm, w_pair.at[pl.ds(0, HD)], load_sem.at[0]),
        pltpu.make_async_copy(wv_hbm, w_pair.at[pl.ds(HD, HD)], load_sem.at[1]),
    ]
    for i in range(parts):
        view = pl.ds(i * part, part)
        loads.append(pltpu.make_async_copy(tokens_hbm.at[view], tokens.at[view], load_sem.at[2 + i]))
    loads.append(pltpu.make_async_copy(wq_hbm, wq, load_sem.at[2 + parts]))
    loads.append(pltpu.make_async_copy(wo_hbm, wo, load_sem.at[3 + parts]))
    for load in loads:
        load.start()

    ask_out[...] = jnp.full(ask_out.shape, -1, jnp.int32)
    ask_out[:, :sel] = chosen_vmem[...]
    asks[...] = jnp.full(asks.shape, -1, jnp.int32)

    barrier = pltpu.get_barrier_semaphore()

    def greet(peer):
        @pl.when(peer != me)
        def _():
            pl.semaphore_signal(barrier, inc=1, device_id=(peer, tp), device_id_type=MESH)

    peer_loop(greet)
    for other in [partner] + far:
        pl.semaphore_signal(barrier, inc=1, device_id=(me, other), device_id_type=MESH)

    pl.semaphore_wait(barrier, n_kv + len(far))

    def ask_copy(source, owner):
        return pltpu.make_async_remote_copy(
            src_ref=ask_out,
            dst_ref=asks.at[source],
            send_sem=ask_send.at[owner],
            recv_sem=ask_recv.at[source],
            device_id=(owner, tp),
            device_id_type=MESH,
        )

    def kv_copy(owner, taker):
        return pltpu.make_async_remote_copy(
            src_ref=kv_out.at[taker],
            dst_ref=kv_in.at[owner],
            send_sem=kv_send.at[taker],
            recv_sem=kv_recv.at[owner],
            device_id=(taker, tp),
            device_id_type=MESH,
        )

    def start_ask(peer):
        @pl.when(peer < me)
        def _():
            ask_copy(me, peer).start()

    peer_loop(start_ask)

    lane = lax.broadcasted_iota(jnp.int32, (BLK, 2 * HD), 1)
    row = lax.broadcasted_iota(jnp.int32, (BLK, 2 * HD), 0)
    low = lane < HD
    first_half = lax.rem(lane, HD) < HD // 2
    sign = jnp.where(first_half, -1.0, 1.0).astype(F32)
    first_row = pl.multiple_of(me * blocks, blocks)
    block_cos = cos_block[pl.ds(first_row, blocks), :]
    block_sin = sin_block[pl.ds(first_row, blocks), :]
    row_cos, row_sin = cos_row[...], sin_row[...]
    for b in range(blocks):
        bc, bs = block_cos[b : b + 1, :], block_sin[b : b + 1, :]
        cos_tab[pl.ds(b * BLK, BLK), :] = bc * row_cos - bs * row_sin
        sin_tab[pl.ds(b * BLK, BLK), :] = (bs * row_cos + bc * row_sin) * sign

    low_f = jnp.where(low, 1.0, 0.0).astype(F32)
    low_b = low_f.astype(BF16)
    high_b = (1.0 - low_f).astype(BF16)
    onehot = jnp.where(lane - HD == row, 1.0, 0.0).astype(F32)
    causal = jnp.where((lane >= HD) & (row > lane - HD), MASKED, 0.0).astype(BF16)
    k_pool[null_id] = jnp.where(low, 0.0, MASKED).astype(BF16)
    v_pool[null_id] = low_b

    def turn(values, c, s):
        width = values.shape[0]
        lanes = lax.broadcasted_iota(jnp.int32, (width, 2 * HD), 1)
        early = lax.rem(lanes, HD) < HD // 2
        swapped = jnp.where(
            early,
            pltpu.roll(values, 2 * HD - HD // 2, 1),
            pltpu.roll(values, HD // 2, 1),
        )
        return values * c + swapped * s

    loads[0].wait()
    loads[1].wait()
    for i in range(parts):
        loads[2 + i].wait()
        pair = lax.dot_general(
            tokens[pl.ds(i * part, part), :],
            w_pair[...],
            (((1,), (1,)), ((), ())),
            preferred_element_type=F32,
        )
        for j in range(part // BLK):
            b = i * (part // BLK) + j
            piece = pair[j * BLK : (j + 1) * BLK, :]
            view = pl.ds(b * BLK, BLK)
            turned = turn(piece, cos_tab[view, :], sin_tab[view, :])
            both = jnp.where(low, turned, piece).astype(BF16)
            kv_local[b] = both
            k_pool[n_kv + b] = both * low_b
            v_pool[n_kv + b] = both * high_b + low_b

    def take_ask(peer):
        @pl.when(peer > me)
        def _():
            ask_copy(peer, me).wait_recv()

    peer_loop(take_ask)

    def fill(peer):
        place = asks[peer] - me * blocks
        inside = (place >= 0) & (place < blocks)
        index = jnp.max(jnp.where(inside, place, 0))
        kv_out[peer] = kv_local[index]

    peer_loop(fill)

    def start_kv(peer):
        @pl.when(peer > me)
        def _():
            kv_copy(me, peer).start()

    peer_loop(start_kv)

    loads[2 + parts].wait()
    q_scale = math.log2(math.e) * HD ** (-0.5)
    for i in range(parts):
        raw = jnp.dot(tokens[pl.ds(i * part, part), :], wq[...], preferred_element_type=F32)
        for j in range(part // BLK):
            b = i * (part // BLK) + j
            view = pl.ds(b * BLK, BLK)
            c, s = cos_tab[view, :] * q_scale, sin_tab[view, :] * q_scale
            for t in range(heads // 2):
                piece = raw[j * BLK : (j + 1) * BLK, t * 2 * HD : (t + 1) * 2 * HD]
                turned = turn(piece, c, s)
                q_stack[b, pl.ds(2 * t * BLK, BLK), :] = jnp.where(low, turned, onehot).astype(BF16)
                q_stack[b, pl.ds((2 * t + 1) * BLK, BLK), :] = jnp.where(
                    low, pltpu.roll(turned, HD, 1), onehot
                ).astype(BF16)

    def take_kv(peer):
        @pl.when(peer < me)
        def _():
            kv_copy(peer, me).wait_recv()
            got = kv_in[peer]
            k_pool[peer] = got * low_b
            v_pool[peer] = got * high_b + low_b

    peer_loop(take_kv)

    def near_copy(c):
        return pltpu.make_async_remote_copy(
            src_ref=gathered.at[tp, c],
            dst_ref=gathered.at[tp, c],
            send_sem=near_send.at[c],
            recv_sem=g_recv.at[tp, c],
            device_id=(me, partner),
            device_id_type=MESH,
        )

    def far_copy(k, c):
        return pltpu.make_async_remote_copy(
            src_ref=gathered.at[tp, c],
            dst_ref=gathered.at[tp, c],
            send_sem=far_send.at[k, c],
            recv_sem=g_recv.at[tp, c],
            device_id=(me, far[k]),
            device_id_type=MESH,
        )

    def relay_copy(k, c):
        return pltpu.make_async_remote_copy(
            src_ref=gathered.at[far[k], c],
            dst_ref=gathered.at[far[k], c],
            send_sem=relay_send.at[k, c],
            recv_sem=g_recv.at[far[k], c],
            device_id=(me, partner),
            device_id_type=MESH,
        )

    def recv_wait(source, c):
        pltpu.make_async_remote_copy(
            src_ref=gathered.at[source, c],
            dst_ref=gathered.at[source, c],
            send_sem=near_send.at[c],
            recv_sem=g_recv.at[source, c],
            device_id=(me, partner),
            device_id_type=MESH,
        ).wait_recv()

    def relay(c):
        for k in range(len(far)):
            recv_wait(far[k], c)
            relay_copy(k, c).start()

    lag = 4
    for b in range(blocks):
        ids = []
        for s in range(sel):
            named = chosen_smem[b, s]
            place = named - me * blocks
            ids.append(
                jnp.where(
                    named < 0,
                    null_id,
                    jnp.where(place >= 0, n_kv + place, lax.div(jnp.maximum(named, 0), blocks)),
                )
            )
        keys = [k_pool[n_kv + b] + causal] + [k_pool[i] for i in ids[1:]]
        values = [v_pool[n_kv + b]] + [v_pool[i] for i in ids[1:]]
        scores = lax.dot_general(
            q_stack[b],
            jnp.concatenate(keys, axis=0),
            (((1,), (1,)), ((), ())),
            preferred_element_type=F32,
        )
        peak = jnp.max(scores, axis=1, keepdims=True)
        weights = jnp.exp2(scores - peak).astype(BF16)
        mixed = jnp.dot(weights, jnp.concatenate(values, axis=0), preferred_element_type=F32)
        rolled = pltpu.roll(mixed, HD, 1)
        for t in range(heads // 2):
            even = slice(2 * t * BLK, (2 * t + 1) * BLK)
            odd = slice((2 * t + 1) * BLK, (2 * t + 2) * BLK)
            top = jnp.where(low, rolled[even, :], mixed[odd, :])
            bottom = jnp.where(low, mixed[even, :], rolled[odd, :])
            gathered[tp, b, :, t * 2 * HD : (t + 1) * 2 * HD] = (top / bottom).astype(BF16)
        for k in range(len(far)):
            far_copy(k, b).start()
        near_copy(b).start()
        if b >= lag:
            relay(b - lag)

    loads[3 + parts].wait()

    def add_source(source, first, count, fresh):
        height = count * BLK
        view = pl.ds(first * BLK, height)
        heads_f = gathered[source, pl.ds(first, count)].reshape(height, feat).astype(F32)
        squared = heads_f * heads_f
        folded = squared[:, : 2 * HD]
        for t in range(1, feat // (2 * HD)):
            folded = folded + squared[:, t * 2 * HD : (t + 1) * 2 * HD]
        start = pl.multiple_of(source * feat, 2 * HD)
        scaled = (heads_f * gain_ref[:, pl.ds(start, feat)]).astype(BF16)
        product = jnp.dot(scaled, wo[pl.ds(start, feat), :], preferred_element_type=F32)
        if fresh:
            sq_acc[view, :] = folded
            acc[view, :] = product
        else:
            sq_acc[view, :] += folded
            acc[view, :] += product

    add_source(tp, 0, blocks, True)
    for c in range(max(blocks - lag, 0), blocks - 2):
        relay(c)
    for c in range(blocks):
        recv_wait(partner, c)
    add_source(partner, 0, blocks, False)
    for c in range(max(blocks - 2, 0), blocks):
        relay(c)

    group = 2
    for g in range(blocks // group):
        for k in range(len(far)):
            add_source(far[k], g * group, group, False)
            mate = far[k] + 1 - 2 * lax.rem(far[k], 2)
            for c in range(g * group, (g + 1) * group):
                recv_wait(mate, c)
            add_source(mate, g * group, group, False)
        view = pl.ds(g * group * BLK, group * BLK)
        inverse = lax.rsqrt(
            jnp.sum(sq_acc[view, :], axis=1, keepdims=True) / total_feat + NORM_EPS
        )
        out_ref[view, :] = (acc[view, :] * inverse).astype(BF16)

    def drain(peer):
        @pl.when(peer < me)
        def _():
            ask_copy(me, peer).wait_send()

        @pl.when(peer > me)
        def _():
            kv_copy(me, peer).wait_send()

    peer_loop(drain)
    for c in range(blocks):
        near_copy(c).wait_send()
        for k in range(len(far)):
            far_copy(k, c).wait_send()
            relay_copy(k, c).wait_send()


def per_device(n_kv, n_tp, tokens, w_query, w_key, w_value, w_out, out_gain, chosen):
    rows, width = tokens.shape
    blocks = rows // BLK
    feat = w_query.shape[1]
    out_cols = w_out.shape[1]
    pool = n_kv + blocks + 1
    cos_block, sin_block = angle_tables(n_kv * blocks, BLK)
    cos_row, sin_row = angle_tables(BLK, 1)
    far = max(n_tp // 2 - 1, 1)
    hbm = pl.BlockSpec(memory_space=pl.ANY)
    vmem = pl.BlockSpec(memory_space=pltpu.VMEM)
    smem = pl.BlockSpec(memory_space=pltpu.SMEM)
    picks = chosen.reshape(blocks, chosen.shape[2])
    dma = pltpu.SemaphoreType.DMA
    return pl.pallas_call(
        functools.partial(kernel, n_kv, n_tp),
        out_shape=jax.ShapeDtypeStruct((rows, out_cols), BF16),
        in_specs=[hbm] * 5 + [vmem, smem, vmem] + [vmem] * 4,
        out_specs=vmem,
        scratch_shapes=[
            pltpu.VMEM(tokens.shape, BF16),
            pltpu.VMEM(w_query.shape, BF16),
            pltpu.VMEM((2 * HD, width), BF16),
            pltpu.VMEM(w_out.shape, BF16),
            pltpu.VMEM((rows, 2 * HD), F32),
            pltpu.VMEM((rows, 2 * HD), F32),
            pltpu.VMEM((blocks, 2 * HD), jnp.int32),
            pltpu.VMEM((n_kv, blocks, 2 * HD), jnp.int32),
            pltpu.VMEM((blocks, BLK, 2 * HD), BF16),
            pltpu.VMEM((n_kv, BLK, 2 * HD), BF16),
            pltpu.VMEM((n_kv, BLK, 2 * HD), BF16),
            pltpu.VMEM((pool, BLK, 2 * HD), BF16),
            pltpu.VMEM((pool, BLK, 2 * HD), BF16),
            pltpu.VMEM((blocks, feat // HD * BLK, 2 * HD), BF16),
            pltpu.VMEM((n_tp, blocks, BLK, feat), BF16),
            pltpu.VMEM((rows, out_cols), F32),
            pltpu.VMEM((rows, 2 * HD), F32),
            dma((6,)),
            dma((n_kv,)),
            dma((n_kv,)),
            dma((n_kv,)),
            dma((n_kv,)),
            dma((blocks,)),
            dma((far, blocks)),
            dma((far, blocks)),
            dma((n_tp, blocks)),
        ],
        compiler_params=pltpu.CompilerParams(collective_id=0, has_side_effects=True),
        name="layer",
    )(
        tokens,
        w_query,
        w_key.T,
        w_value.T,
        w_out,
        out_gain.reshape(1, -1),
        picks,
        picks,
        cos_block,
        sin_block,
        cos_row,
        sin_row,
    )


def solution(mesh):
    return jax.shard_map(
        functools.partial(per_device, mesh.shape["kv"], mesh.shape["tp"]),
        mesh=mesh,
        in_specs=(
            P("kv", None),
            P(None, "tp"),
            P(None, "tp"),
            P(None, "tp"),
            P(None, "tp"),
            P(),
            P("tp", "kv", None),
        ),
        out_specs=P("kv", "tp"),
        check_vma=False,
    )
```

time: 87.9 us -> 25.5 us (0.29)
  the two profiles are of different devices: /device:TPU:0 before, /device:TPU:25 now
where the time goes in v1:
time: 25.5 us; the launch traced here: 25.2 us
  Pallas kernels  23.3 us (91%)
  local copies, waits for them, and re-layouts  1.87 us (7%)
    pallas_call x1, Pallas kernels, per_device(): pl.pallas_call(functools.partial(kernel, n_kv, n_tp), out_shape=jax.Shape...  23.3 us
    unnamed x1, local copies, waits for them, and re-layouts  1.87 us

profile of v1, /device:TPU:25, one launch (start us, length us, event | category | flops | bytes accessed | tf_op | source)
XLA Modules:
  0.0 25.2 jit_solution(17915265502873738920)
XLA Ops:
  0.0 23.3 %layer.1 = bf16[512,512]{1,0:T(8,128)(2,1)} custom-call(bf16[512,2048]{1,0:T(8,128)(2,1)} %tokens_hbm.1, bf16[2048,256]{1,0:T(8,128)(2,1)} %wq_hbm.1, bf16[64,2048]{1,0:T(8,128)(2,1)} %bitcast.4, bf16[64,2048]{1,0:T(8,128)(2,1)} %bitcast.5, bf16[1024,512]{1,0:T(8,128)(2,1)} %wo_hbm.1, f32[1,1024]{1,0:T(1,128)} %bitcast.8, s32[8,8]{1,0:T(8,128)} %bitcast.6, ...), custom_call_target="tpu_custom_call" | custom-call | tf_op jit(solution)/shard_map/layer/pallas_call | solution.py:411
  23.3 1.9 %copy.13 = bf16[512,512]{1,0:T(8,128)(2,1)} copy(bf16[512,512]{1,0:T(8,128)(2,1)} %layer.1) | data formatting | bytes 1048576

commit v2 on v1

--- a/solution.py
+++ b/solution.py
@@ -35,14 +35,16 @@
     wk_hbm,
     wv_hbm,
     wo_hbm,
+    gain_hbm,
+    chosen_hbm,
+    block_hbm,
+    row_hbm,
+    out_ref,
     gain_ref,
     chosen_smem,
     chosen_vmem,
-    cos_block,
-    sin_block,
-    cos_row,
-    sin_row,
-    out_ref,
+    block_tab,
+    row_tab,
     tokens,
     wq,
     w_pair,
@@ -95,34 +97,37 @@
             def _(peer):
                 body(peer)
 
-    loads = [
-        pltpu.make_async_copy(wk_hbm, w_pair.at[pl.ds(0, HD)], load_sem.at[0]),
-        pltpu.make_async_copy(wv_hbm, w_pair.at[pl.ds(HD, HD)], load_sem.at[1]),
+    asks[...] = jnp.full(asks.shape, -1, jnp.int32)
+    barrier = pltpu.get_barrier_semaphore()
+
+    def greet(peer):
+        @pl.when(peer != me)
+        def _():
+            pl.semaphore_signal(barrier, inc=1, device_id=(peer, tp), device_id_type=MESH)
+
+    peer_loop(greet)
+    for other in [partner] + far:
+        pl.semaphore_signal(barrier, inc=1, device_id=(me, other), device_id_type=MESH)
+
+    first_block = pl.multiple_of(me * blocks, blocks)
+    pairs = [
+        (block_hbm.at[:, pl.ds(first_block, blocks)], block_tab),
+        (row_hbm, row_tab),
+        (chosen_hbm, chosen_vmem),
+        (chosen_hbm, chosen_smem),
+        (wk_hbm, w_pair.at[pl.ds(0, HD)]),
+        (wv_hbm, w_pair.at[pl.ds(HD, HD)]),
     ]
     for i in range(parts):
         view = pl.ds(i * part, part)
-        loads.append(pltpu.make_async_copy(tokens_hbm.at[view], tokens.at[view], load_sem.at[2 + i]))
-    loads.append(pltpu.make_async_copy(wq_hbm, wq, load_sem.at[2 + parts]))
-    loads.append(pltpu.make_async_copy(wo_hbm, wo, load_sem.at[3 + parts]))
+        pairs.append((tokens_hbm.at[view], tokens.at[view]))
+    pairs += [(wq_hbm, wq), (gain_hbm, gain_ref), (wo_hbm, wo)]
+    loads = [
+        pltpu.make_async_copy(source, target, load_sem.at[n])
+        for n, (source, target) in enumerate(pairs)
+    ]
     for load in loads:
         load.start()
-
-    ask_out[...] = jnp.full(ask_out.shape, -1, jnp.int32)
-    ask_out[:, :sel] = chosen_vmem[...]
-    asks[...] = jnp.full(asks.shape, -1, jnp.int32)
-
-    barrier = pltpu.get_barrier_semaphore()
-
-    def greet(peer):
-        @pl.when(peer != me)
-        def _():
-            pl.semaphore_signal(barrier, inc=1, device_id=(peer, tp), device_id_type=MESH)
-
-    peer_loop(greet)
-    for other in [partner] + far:
-        pl.semaphore_signal(barrier, inc=1, device_id=(me, other), device_id_type=MESH)
-
-    pl.semaphore_wait(barrier, n_kv + len(far))
 
     def ask_copy(source, owner):
         return pltpu.make_async_remote_copy(
@@ -144,22 +149,15 @@
             device_id_type=MESH,
         )
 
-    def start_ask(peer):
-        @pl.when(peer < me)
-        def _():
-            ask_copy(me, peer).start()
-
-    peer_loop(start_ask)
-
     lane = lax.broadcasted_iota(jnp.int32, (BLK, 2 * HD), 1)
     row = lax.broadcasted_iota(jnp.int32, (BLK, 2 * HD), 0)
     low = lane < HD
     first_half = lax.rem(lane, HD) < HD // 2
     sign = jnp.where(first_half, -1.0, 1.0).astype(F32)
-    first_row = pl.multiple_of(me * blocks, blocks)
-    block_cos = cos_block[pl.ds(first_row, blocks), :]
-    block_sin = sin_block[pl.ds(first_row, blocks), :]
-    row_cos, row_sin = cos_row[...], sin_row[...]
+    loads[0].wait()
+    loads[1].wait()
+    block_cos, block_sin = block_tab[0], block_tab[1]
+    row_cos, row_sin = row_tab[0], row_tab[1]
     for b in range(blocks):
         bc, bs = block_cos[b : b + 1, :], block_sin[b : b + 1, :]
         cos_tab[pl.ds(b * BLK, BLK), :] = bc * row_cos - bs * row_sin
@@ -184,10 +182,10 @@
         )
         return values * c + swapped * s
 
-    loads[0].wait()
-    loads[1].wait()
+    loads[4].wait()
+    loads[5].wait()
     for i in range(parts):
-        loads[2 + i].wait()
+        loads[6 + i].wait()
         pair = lax.dot_general(
             tokens[pl.ds(i * part, part), :],
             w_pair[...],
@@ -204,29 +202,7 @@
             k_pool[n_kv + b] = both * low_b
             v_pool[n_kv + b] = both * high_b + low_b
 
-    def take_ask(peer):
-        @pl.when(peer > me)
-        def _():
-            ask_copy(peer, me).wait_recv()
-
-    peer_loop(take_ask)
-
-    def fill(peer):
-        place = asks[peer] - me * blocks
-        inside = (place >= 0) & (place < blocks)
-        index = jnp.max(jnp.where(inside, place, 0))
-        kv_out[peer] = kv_local[index]
-
-    peer_loop(fill)
-
-    def start_kv(peer):
-        @pl.when(peer > me)
-        def _():
-            kv_copy(me, peer).start()
-
-    peer_loop(start_kv)
-
-    loads[2 + parts].wait()
+    loads[6 + parts].wait()
     q_scale = math.log2(math.e) * HD ** (-0.5)
     for i in range(parts):
         raw = jnp.dot(tokens[pl.ds(i * part, part), :], wq[...], preferred_element_type=F32)
@@ -242,6 +218,31 @@
                     low, pltpu.roll(turned, HD, 1), onehot
                 ).astype(BF16)
 
+    loads[2].wait()
+    loads[3].wait()
+    ask_out[...] = jnp.full(ask_out.shape, -1, jnp.int32)
+    ask_out[:, :sel] = chosen_vmem[...]
+    pl.semaphore_wait(barrier, n_kv + len(far))
+
+    def start_ask(peer):
+        @pl.when(peer < me)
+        def _():
+            ask_copy(me, peer).start()
+
+    peer_loop(start_ask)
+
+    def answer(peer):
+        @pl.when(peer > me)
+        def _():
+            ask_copy(peer, me).wait_recv()
+            place = asks[peer] - me * blocks
+            inside = (place >= 0) & (place < blocks)
+            index = jnp.max(jnp.where(inside, place, 0))
+            kv_out[peer] = kv_local[index]
+            kv_copy(me, peer).start()
+
+    peer_loop(answer)
+
     def take_kv(peer):
         @pl.when(peer < me)
         def _():
@@ -250,7 +251,7 @@
             k_pool[peer] = got * low_b
             v_pool[peer] = got * high_b + low_b
 
-    peer_loop(take_kv)
+    peer_loop(lambda peer: take_kv(n_kv - 1 - peer))
 
     def near_copy(c):
         return pltpu.make_async_remote_copy(
@@ -297,7 +298,6 @@
             recv_wait(far[k], c)
             relay_copy(k, c).start()
 
-    lag = 4
     for b in range(blocks):
         ids = []
         for s in range(sel):
@@ -331,10 +331,9 @@
         for k in range(len(far)):
             far_copy(k, b).start()
         near_copy(b).start()
-        if b >= lag:
-            relay(b - lag)
-
-    loads[3 + parts].wait()
+
+    loads[7 + parts].wait()
+    loads[8 + parts].wait()
 
     def add_source(source, first, count, fresh):
         height = count * BLK
@@ -354,28 +353,28 @@
             sq_acc[view, :] += folded
             acc[view, :] += product
 
-    add_source(tp, 0, blocks, True)
-    for c in range(max(blocks - lag, 0), blocks - 2):
-        relay(c)
-    for c in range(blocks):
+    def finish(c):
+        view = pl.ds(c * BLK, BLK)
         recv_wait(partner, c)
-    add_source(partner, 0, blocks, False)
-    for c in range(max(blocks - 2, 0), blocks):
-        relay(c)
-
-    group = 2
-    for g in range(blocks // group):
+        add_source(partner, c, 1, False)
         for k in range(len(far)):
-            add_source(far[k], g * group, group, False)
             mate = far[k] + 1 - 2 * lax.rem(far[k], 2)
-            for c in range(g * group, (g + 1) * group):
-                recv_wait(mate, c)
-            add_source(mate, g * group, group, False)
-        view = pl.ds(g * group * BLK, group * BLK)
+            recv_wait(mate, c)
+            add_source(mate, c, 1, False)
         inverse = lax.rsqrt(
             jnp.sum(sq_acc[view, :], axis=1, keepdims=True) / total_feat + NORM_EPS
         )
         out_ref[view, :] = (acc[view, :] * inverse).astype(BF16)
+
+    add_source(tp, 0, blocks, True)
+    lag = 2
+    for c in range(blocks + lag):
+        if c < blocks:
+            relay(c)
+            for k in range(len(far)):
+                add_source(far[k], c, 1, False)
+        if c >= lag:
+            finish(c - lag)
 
     def drain(peer):
         @pl.when(peer < me)
@@ -400,20 +399,24 @@
     feat = w_query.shape[1]
     out_cols = w_out.shape[1]
     pool = n_kv + blocks + 1
-    cos_block, sin_block = angle_tables(n_kv * blocks, BLK)
-    cos_row, sin_row = angle_tables(BLK, 1)
+    block_table = np.stack(angle_tables(n_kv * blocks, BLK))
+    row_table = np.stack(angle_tables(BLK, 1))
     far = max(n_tp // 2 - 1, 1)
     hbm = pl.BlockSpec(memory_space=pl.ANY)
     vmem = pl.BlockSpec(memory_space=pltpu.VMEM)
-    smem = pl.BlockSpec(memory_space=pltpu.SMEM)
     picks = chosen.reshape(blocks, chosen.shape[2])
     dma = pltpu.SemaphoreType.DMA
     return pl.pallas_call(
         functools.partial(kernel, n_kv, n_tp),
-        out_shape=jax.ShapeDtypeStruct((rows, out_cols), BF16),
-        in_specs=[hbm] * 5 + [vmem, smem, vmem] + [vmem] * 4,
+        out_shape=pltpu.VMEM((rows, out_cols), BF16),
+        in_specs=[hbm] * 9,
         out_specs=vmem,
         scratch_shapes=[
+            pltpu.VMEM((1, out_gain.shape[0]), F32),
+            pltpu.SMEM(picks.shape, jnp.int32),
+            pltpu.VMEM(picks.shape, jnp.int32),
+            pltpu.VMEM((2, blocks, 2 * HD), F32),
+            pltpu.VMEM((2, BLK, 2 * HD), F32),
             pltpu.VMEM(tokens.shape, BF16),
             pltpu.VMEM(w_query.shape, BF16),
             pltpu.VMEM((2 * HD, width), BF16),
@@ -431,7 +434,7 @@
             pltpu.VMEM((n_tp, blocks, BLK, feat), BF16),
             pltpu.VMEM((rows, out_cols), F32),
             pltpu.VMEM((rows, 2 * HD), F32),
-            dma((6,)),
+            dma((11,)),
             dma((n_kv,)),
             dma((n_kv,)),
             dma((n_kv,)),
@@ -451,11 +454,8 @@
         w_out,
         out_gain.reshape(1, -1),
         picks,
-        picks,
-        cos_block,
-        sin_block,
-        cos_row,
-        sin_row,
+        block_table,
+        row_table,
     )
 
 

time: 25.5 us -> 23.5 us (0.922)
  local copies, waits for them, and re-layouts: 1.87 us -> 0.8 us
  Pallas kernels: 23.3 us -> 22.5 us
    unnamed x1, local copies, waits for them, and re-layouts: 1.87 us -> 0.8 us
    pallas_call x1, Pallas kernels: 23.3 us -> 22.5 us  [per_device(): pl.pallas_call(functools.partial(kernel, n_kv, n_tp), out_shape=pltpu.VME...]
where the time goes in v2:
time: 23.5 us; the launch traced here: 23.3 us
  Pallas kernels  22.5 us (96%)
  local copies, waits for them, and re-layouts  0.8 us (3%)
    pallas_call x1, Pallas kernels, per_device(): pl.pallas_call(functools.partial(kernel, n_kv, n_tp), out_shape=pltpu.VME...  22.5 us
    unnamed x1, local copies, waits for them, and re-layouts  0.8 us

profile of v2, /device:TPU:25, one launch (start us, length us, event | category | flops | bytes accessed | tf_op | source)
XLA Modules:
  0.0 23.3 jit_solution(9468008218079840341)
XLA Ops:
  0.0 22.5 %layer.1 = bf16[512,512]{1,0:T(8,128)(2,1)S(1)} custom-call(bf16[512,2048]{1,0:T(8,128)(2,1)} %tokens_hbm.1, bf16[2048,256]{1,0:T(8,128)(2,1)} %wq_hbm.1, bf16[64,2048]{1,0:T(8,128)(2,1)} %bitcast.4, bf16[64,2048]{1,0:T(8,128)(2,1)} %bitcast.5, bf16[1024,512]{1,0:T(8,128)(2,1)} %wo_hbm.1, f32[1,1024]{1,0:T(1,128)} %bitcast.6, s32[8,8]{1,0:T(8,128)} %bitcast.7, ...), custom_call_target="tpu_custom_call" | custom-call | tf_op jit(solution)/shard_map/layer/pallas_call | solution.py:409
  22.5 0.8 %copy.11 = bf16[512,512]{1,0:T(8,128)(2,1)} copy(bf16[512,512]{1,0:T(8,128)(2,1)S(1)} %layer.1) | data formatting | bytes 1048576

commit v3 on v2

--- a/solution.py
+++ b/solution.py
@@ -14,6 +14,7 @@
 ROPE_BASE = 500000.0
 NORM_EPS = 1e-06
 MASKED = -1e30
+GROUP = 2
 MESH = pl.DeviceIdType.MESH
 F32 = jnp.float32
 BF16 = jnp.bfloat16
@@ -253,10 +254,13 @@
 
     peer_loop(lambda peer: take_kv(n_kv - 1 - peer))
 
+    group = math.gcd(GROUP, blocks)
+    chunks = blocks // group
+
     def near_copy(c):
         return pltpu.make_async_remote_copy(
-            src_ref=gathered.at[tp, c],
-            dst_ref=gathered.at[tp, c],
+            src_ref=gathered.at[tp, pl.ds(c * group, group)],
+            dst_ref=gathered.at[tp, pl.ds(c * group, group)],
             send_sem=near_send.at[c],
             recv_sem=g_recv.at[tp, c],
             device_id=(me, partner),
@@ -265,8 +269,8 @@
 
     def far_copy(k, c):
         return pltpu.make_async_remote_copy(
-            src_ref=gathered.at[tp, c],
-            dst_ref=gathered.at[tp, c],
+            src_ref=gathered.at[tp, pl.ds(c * group, group)],
+            dst_ref=gathered.at[tp, pl.ds(c * group, group)],
             send_sem=far_send.at[k, c],
             recv_sem=g_recv.at[tp, c],
             device_id=(me, far[k]),
@@ -275,8 +279,8 @@
 
     def relay_copy(k, c):
         return pltpu.make_async_remote_copy(
-            src_ref=gathered.at[far[k], c],
-            dst_ref=gathered.at[far[k], c],
+            src_ref=gathered.at[far[k], pl.ds(c * group, group)],
+            dst_ref=gathered.at[far[k], pl.ds(c * group, group)],
             send_sem=relay_send.at[k, c],
             recv_sem=g_recv.at[far[k], c],
             device_id=(me, partner),
@@ -285,8 +289,8 @@
 
     def recv_wait(source, c):
         pltpu.make_async_remote_copy(
-            src_ref=gathered.at[source, c],
-            dst_ref=gathered.at[source, c],
+            src_ref=gathered.at[source, pl.ds(c * group, group)],
+            dst_ref=gathered.at[source, pl.ds(c * group, group)],
             send_sem=near_send.at[c],
             recv_sem=g_recv.at[source, c],
             device_id=(me, partner),
@@ -328,9 +332,10 @@
             top = jnp.where(low, rolled[even, :], mixed[odd, :])
             bottom = jnp.where(low, mixed[even, :], rolled[odd, :])
             gathered[tp, b, :, t * 2 * HD : (t + 1) * 2 * HD] = (top / bottom).astype(BF16)
-        for k in range(len(far)):
-            far_copy(k, b).start()
-        near_copy(b).start()
+        if (b + 1) % group == 0:
+            for k in range(len(far)):
+                far_copy(k, b // group).start()
+            near_copy(b // group).start()
 
     loads[7 + parts].wait()
     loads[8 + parts].wait()
@@ -354,25 +359,30 @@
             acc[view, :] += product
 
     def finish(c):
-        view = pl.ds(c * BLK, BLK)
-        recv_wait(partner, c)
-        add_source(partner, c, 1, False)
+        view = pl.ds(c * group * BLK, group * BLK)
         for k in range(len(far)):
             mate = far[k] + 1 - 2 * lax.rem(far[k], 2)
             recv_wait(mate, c)
-            add_source(mate, c, 1, False)
+            add_source(mate, c * group, group, False)
         inverse = lax.rsqrt(
             jnp.sum(sq_acc[view, :], axis=1, keepdims=True) / total_feat + NORM_EPS
         )
         out_ref[view, :] = (acc[view, :] * inverse).astype(BF16)
 
     add_source(tp, 0, blocks, True)
-    lag = 2
-    for c in range(blocks + lag):
-        if c < blocks:
-            relay(c)
+    early = 1
+    for c in range(early):
+        relay(c)
+    for c in range(chunks):
+        recv_wait(partner, c)
+    add_source(partner, 0, blocks, False)
+    lag = 1
+    for c in range(chunks + lag):
+        if c < chunks:
+            if c >= early:
+                relay(c)
             for k in range(len(far)):
-                add_source(far[k], c, 1, False)
+                add_source(far[k], c * group, group, False)
         if c >= lag:
             finish(c - lag)
 
@@ -386,7 +396,7 @@
             kv_copy(me, peer).wait_send()
 
     peer_loop(drain)
-    for c in range(blocks):
+    for c in range(chunks):
         near_copy(c).wait_send()
         for k in range(len(far)):
             far_copy(k, c).wait_send()

time: 23.5 us -> 23.2 us (0.987)
    pallas_call x1, Pallas kernels: 22.5 us -> 22.3 us  [per_device(): pl.pallas_call(functools.partial(kernel, n_kv, n_tp), out_shape=pltpu.VME...]
where the time goes in v3:
time: 23.2 us; the launch traced here: 23.1 us
  Pallas kernels  22.3 us (96%)
  local copies, waits for them, and re-layouts  0.8 us (3%)
    pallas_call x1, Pallas kernels, per_device(): pl.pallas_call(functools.partial(kernel, n_kv, n_tp), out_shape=pltpu.VME...  22.3 us
    unnamed x1, local copies, waits for them, and re-layouts  0.8 us

profile of v3, /device:TPU:25, one launch (start us, length us, event | category | flops | bytes accessed | tf_op | source)
XLA Modules:
  0.0 23.1 jit_solution(15317525842180052384)
XLA Ops:
  0.0 22.3 %layer.1 = bf16[512,512]{1,0:T(8,128)(2,1)S(1)} custom-call(bf16[512,2048]{1,0:T(8,128)(2,1)} %tokens_hbm.1, bf16[2048,256]{1,0:T(8,128)(2,1)} %wq_hbm.1, bf16[64,2048]{1,0:T(8,128)(2,1)} %bitcast.4, bf16[64,2048]{1,0:T(8,128)(2,1)} %bitcast.5, bf16[1024,512]{1,0:T(8,128)(2,1)} %wo_hbm.1, f32[1,1024]{1,0:T(1,128)} %bitcast.6, s32[8,8]{1,0:T(8,128)} %bitcast.7, ...), custom_call_target="tpu_custom_call" | custom-call | tf_op jit(solution)/shard_map/layer/pallas_call | solution.py:419
  22.3 0.8 %copy.11 = bf16[512,512]{1,0:T(8,128)(2,1)} copy(bf16[512,512]{1,0:T(8,128)(2,1)S(1)} %layer.1) | data formatting | bytes 1048576
